TPU v7x, 256 devices: a whole 4x4x8 slice. The times are simulated.
256 devices in a mesh: sp: 32 (over z, x), tp: 8 (over y, core).
Axes of the slice: x: 4, y: 4, z: 8, core: 2. Of those that a mesh axis runs over, the one named last changes fastest.
Arguments:
- tokens: bfloat16 [12288, 2048], P('sp', 'tp'), may hold values from -6 to 6
- ret_query: bfloat16 [2048, 1024], P(None, 'tp'), may hold values from -0.125 to 0.125
- ret_key: bfloat16 [2048, 1024], P(None, 'tp'), may hold values from -0.125 to 0.125
- ret_value: bfloat16 [2048, 1024], P(None, 'tp'), may hold values from -0.125 to 0.125
- stick_query: bfloat16 [2048, 1024], P(None, 'tp'), may hold values from -0.125 to 0.125
- stick_key: bfloat16 [2048, 1024], P(None, 'tp'), may hold values from -0.125 to 0.125
- stick_value: bfloat16 [2048, 1024], P(None, 'tp'), may hold values from -0.125 to 0.125
- log_decay: float32 [12288, 8], P('sp', 'tp'), may hold values from -1.2 to 0
- stick_bias: float32 [8], P('tp'), may hold values from -13 to -5
- out_ret: bfloat16 [1024, 2048], P('tp'), may hold values from -0.125 to 0.125
- out_stick: bfloat16 [1024, 2048], P('tp'), may hold values from -0.125 to 0.125
Outputs:
- mixed: bfloat16 [12288, 2048], P('sp', 'tp')
All inputs are finite; a program needn't handle non-finite values.
Results may differ from a plain program's by a relative error of at most 0.019.
Values may be sent and summed in bfloat16 or wider, within the bound.
A program may use at most 64 MiB of HBM per device.

v0:
```python
import jax
import jax.numpy as jnp
from jax import lax
from jax.sharding import Mesh
from jax.sharding import PartitionSpec as P

HEAD_DIM = 128
SP = ("sp_0", "sp_1")


EPS = 1e-05
ROPE_BASE = 10000.0


def in_order(pieces, dim):
    dims = list(pieces.shape[1:])
    dims[dim] *= pieces.shape[0]
    return jnp.moveaxis(pieces, 0, dim).reshape(dims)


def from_everyone(array, axis):
    size = lax.axis_size(axis)
    return lax.all_to_all(
        jnp.broadcast_to(array[None], (size, *array.shape)), axis, 0, 0, tiled=True
    )


def collect(array, axis, dim):
    return in_order(from_everyone(array, axis), dim)


def filled_with(array, identity):
    return jax.tree.map(
        lambda part, zero: jnp.zeros_like(part) + jnp.asarray(zero, part.dtype), array, identity
    )


def gathered_once(array, axis):
    leaves = jax.tree.leaves(array)
    sequence = sorted(range(len(leaves)), key=lambda k: -leaves[k].size)
    width = (1, *leaves[sequence[0]].shape)[-1]
    lines = [
        jnp.pad(leaves[k].reshape(-1), (0, -leaves[k].size % width)).reshape(-1, width)
        for k in sequence
    ]
    both, at, found = (lax.all_gather(jnp.concatenate(lines), axis), 0, {})
    for k, line in zip(sequence, lines):
        share = both[:, at : at + len(line)].reshape(len(both), -1)
        found[k] = share[:, : leaves[k].size].reshape(-1, *leaves[k].shape)
        at += len(line)
    numbers = iter(range(len(leaves)))
    return jax.tree.map(lambda _: found[next(numbers)], array)


def carried_in(array, axes, combine, identity):
    before = start = filled_with(array, identity)
    subtotal = array
    for axis in reversed(axes):
        size, position = (lax.axis_size(axis), lax.axis_index(axis))
        pieces = gathered_once(
            jax.tree.map(
                lambda part, kind: part.astype(kind), subtotal, (jnp.bfloat16, jnp.bfloat16)
            ),
            axis,
        )
        inside, subtotal = (start, start)
        for k in range(size):
            passed = k < position
            subtotal = combine(
                subtotal, jax.tree.map(lambda part, own: part[k].astype(own.dtype), pieces, array)
            )
            inside = jax.tree.map(lambda new, old: jnp.where(passed, new, old), subtotal, inside)
        before = combine(inside, before)
    return before


def split_up(array, dim, size):
    before, after = (array.shape[:dim], array.shape[dim + 1 :])
    return jnp.moveaxis(array.reshape(*before, size, -1, *after), dim, 0)


def sent_and_summed(array, axis, dim):
    pieces = split_up(array, dim, lax.axis_size(axis))
    arrived = lax.all_to_all(pieces, axis, split_axis=0, concat_axis=0, tiled=True)
    return arrived.astype(jnp.float32).sum(axis=0)


def rotate(values, positions):
    half_width = values.shape[-1] // 2
    inverse = ROPE_BASE ** (-jnp.arange(half_width, dtype=jnp.float32) / half_width)
    angles = positions[:, None] * inverse[None, :]
    cosine = jnp.cos(angles)[:, None, :]
    sine_part = jnp.sin(angles)[:, None, :]
    first_half = values[..., :half_width]
    second_half = values[..., half_width:]
    return jnp.concatenate(
        [
            first_half * cosine - second_half * sine_part,
            first_half * sine_part + second_half * cosine,
        ],
        axis=-1,
    )


def head_norm(values):
    centred = values - jnp.mean(values, axis=-1, keepdims=True)
    spread = jnp.mean(centred * centred, axis=-1, keepdims=True)
    return centred * lax.rsqrt(spread + EPS)


def chain(earlier, later):
    return (earlier[0] * later[0], later[0][:, None, None] * earlier[1] + later[1])


def group_size(shards, rows):
    chosen = 1
    for count in range(1, min(8, shards) + 1):
        if shards % count == 0 and count * rows <= max(2048, rows):
            chosen = count
    return chosen


def stick_group(queries, key_pairs, bias, query_pos, key_start, shard_rows, running, trailing):
    scale = queries.shape[2] ** (-0.5)
    span_rows = key_pairs.shape[1]
    shard_count = span_rows // shard_rows
    head_count = queries.shape[1]
    key_pos = key_start + jnp.arange(span_rows, dtype=jnp.int32)
    visible = ((key_pos[None, :] >= 0) & (key_pos[None, :] < query_pos[:, None])).reshape(
        1, -1, shard_count, shard_rows
    )
    logits = (
        jnp.einsum("thd,shd->hts", queries, key_pairs[0], preferred_element_type=jnp.float32)
        * scale
        + bias[:, None, None]
    )
    logits = logits.reshape(head_count, -1, shard_count, shard_rows)
    success = jax.nn.log_sigmoid(logits)
    failure = jnp.where(visible, success - logits, 0.0)
    shard_index = jnp.arange(shard_rows, dtype=jnp.int32)
    strictly_after = (shard_index[:, None] > shard_index[None, :]).astype(jnp.float32)
    suffix = jnp.einsum("htgj,jr->htgr", failure, strictly_after)
    weights = jnp.where(visible, jnp.exp(success + suffix), 0.0).astype(jnp.bfloat16)
    value_groups = key_pairs[1].reshape(shard_count, shard_rows, head_count, -1)
    partial_value = jnp.einsum(
        "htgs,gshe->thge", weights, value_groups, preferred_element_type=jnp.float32
    )
    totals = jnp.transpose(jnp.sum(failure, axis=3), (1, 0, 2))
    behind = lax.cumsum(totals, axis=2, reverse=True) - totals + trailing[:, :, None]
    running = running + jnp.sum(jnp.exp(behind)[:, :, :, None] * partial_value, axis=2)
    return (running, trailing + jnp.sum(totals, axis=2))


def body(
    tokens,
    ret_query,
    ret_key,
    ret_value,
    stick_query,
    stick_key,
    stick_value,
    log_decay,
    stick_bias,
    out_ret,
    out_stick,
):
    row_count = tokens.shape[0]
    matrices = (ret_query, ret_key, ret_value, stick_query, stick_key, stick_value)
    piece = collect(tokens, "tp", 1)
    sums = tuple(
        (jnp.dot(piece, matrix, preferred_element_type=jnp.float32) for matrix in matrices)
    )
    ret_q, ret_k, ret_v, stick_q, stick_k, stick_v = [
        total.astype(jnp.bfloat16).reshape(row_count, -1, HEAD_DIM) for total in sums
    ]
    own_index = lax.axis_index(SP)
    positions_int = own_index * row_count + jnp.arange(row_count, dtype=jnp.int32)
    positions = positions_int.astype(jnp.float32)
    query_rot = rotate(ret_q.astype(jnp.float32), positions).astype(jnp.bfloat16)
    key_rot = (rotate(ret_k.astype(jnp.float32), positions) * HEAD_DIM ** (-0.5)).astype(
        jnp.bfloat16
    )
    cumulative = jnp.cumsum(log_decay, axis=0)
    final_decay = cumulative[-1]
    index_rows = jnp.arange(row_count, dtype=jnp.int32)
    lower = (index_rows[:, None] >= index_rows[None, :])[None]
    gaps = cumulative.T[:, :, None] - cumulative.T[:, None, :]
    decay = jnp.where(lower, jnp.exp(jnp.where(lower, gaps, 0.0)), 0.0)
    scores = jnp.einsum("thd,shd->hts", query_rot, key_rot, preferred_element_type=jnp.float32)
    inner = (scores * decay).astype(jnp.bfloat16)
    local_part = jnp.einsum("hts,she->the", inner, ret_v, preferred_element_type=jnp.float32)
    weighted = (
        key_rot.astype(jnp.float32) * jnp.exp(final_decay[None, :] - cumulative)[:, :, None]
    ).astype(jnp.bfloat16)
    fresh = jnp.einsum("shd,she->hde", weighted, ret_v, preferred_element_type=jnp.float32)
    start_pair = (jnp.ones((fresh.shape[0],), jnp.float32), jnp.zeros_like(fresh))
    incoming = carried_in((jnp.exp(final_decay), fresh), SP, chain, start_pair)
    carried = (
        jnp.einsum("thd,hde->the", query_rot.astype(jnp.float32), incoming[1])
        * jnp.exp(cumulative)[:, :, None]
    )
    ret_out = head_norm(local_part + carried).astype(jnp.bfloat16)
    stick_pairs = jnp.stack([stick_k, stick_v])
    shard_total = lax.axis_size(SP)
    per_group = group_size(shard_total, row_count)
    group_count = shard_total // per_group
    start_running = jnp.zeros(stick_q.shape, jnp.float32)
    start_trailing = jnp.zeros((row_count, stick_q.shape[1]), jnp.float32)

    def visit(key_pairs, key_start, running, trailing):
        return stick_group(
            stick_q, key_pairs, stick_bias, positions_int, key_start, row_count, running, trailing
        )

    def unchanged(key_pairs, key_start, running, trailing):
        return (running, trailing)

    every_pair = lax.all_gather(stick_pairs, SP, axis=1, tiled=True)

    def turn(step, carry):
        running, trailing = carry
        group_index = own_index // per_group - step
        key_start = jnp.maximum(group_index, 0) * per_group * row_count
        key_pairs = lax.dynamic_slice_in_dim(every_pair, key_start, per_group * row_count, 1)
        return lax.cond(group_index >= 0, visit, unchanged, key_pairs, key_start, running, trailing)

    gathered_out, behind = lax.fori_loop(0, group_count, turn, (start_running, start_trailing))
    stick_out = head_norm(gathered_out).astype(jnp.bfloat16)
    ret_flat = ret_out.reshape(row_count, -1)
    stick_flat = stick_out.reshape(row_count, -1)
    mixed = sent_and_summed(
        (
            jnp.einsum("tf,fc->ct", ret_flat, out_ret, preferred_element_type=jnp.float32)
            + jnp.einsum("tf,fc->ct", stick_flat, out_stick, preferred_element_type=jnp.float32)
        ).astype(jnp.bfloat16),
        "tp",
        0,
    ).T
    return mixed.astype(jnp.bfloat16)


def solution(mesh):
    split = Mesh(mesh.devices.reshape(8, 4, mesh.shape["tp"]), ("sp_0", "sp_1", "tp"))
    return jax.shard_map(
        body,
        mesh=split,
        in_specs=(
            P(SP, "tp"),
            P(None, "tp"),
            P(None, "tp"),
            P(None, "tp"),
            P(None, "tp"),
            P(None, "tp"),
            P(None, "tp"),
            P(SP, "tp"),
            P("tp"),
            P("tp", None),
            P("tp", None),
        ),
        out_specs=P(SP, "tp"),
        check_vma=False,
    )
```

profile of v0, /device:TPU:224, one launch (start us, length us, event | category | flops | bytes accessed | tf_op | source)
XLA Modules:
  0.0 288.9 jit_solution(1095954268528542361)
XLA Ops:
  7.9 26.0 %all_to_all.10 = bf16[8,384,256]{1,2,0:T(8,128)(2,1)S(1)} all-to-all(bf16[8,384,256]{1,2,0:T(8,128)(2,1)S(1)} %broadcast_in_dim.14), channel_id=1, replica_groups=mesh['sp_0'=8,'sp_1'=4,'tp'=8] {'tp'}, dimensions={0} | all-to-all | bytes 3145728 | tf_op jit(solution)/shard_map/all_to_all | solution.py:23
  41.8 12.7 %all-gather.2 = bf16[4,129,128]{2,1,0:T(8,128)(2,1)S(1)} all-gather(bf16[1,129,128]{2,1,0:T(8,128)(2,1)S(1)} %maximum_bitcast_fusion), channel_id=2, replica_groups=mesh['sp_0'=8,'sp_1'=4,'tp'=8] {'sp_1'}, dimensions={0}, use_global_device_ids=true | all-gather | bytes 165120 | tf_op jit(solution)/shard_map/all_gather | solution.py:46
  58.3 25.1 %all-gather.3 = bf16[8,129,128]{2,1,0:T(8,128)(2,1)S(1)} all-gather(bf16[1,129,128]{2,1,0:T(8,128)(2,1)S(1)} %maximum_bitcast_fusion.1), channel_id=3, replica_groups=mesh['sp_0'=8,'sp_1'=4,'tp'=8] {'sp_0'}, dimensions={0}, use_global_device_ids=true | all-gather | bytes 297216 | tf_op jit(solution)/shard_map/all_gather | solution.py:46
  92.9 2.3 fusion.88
  95.2 26.1 %all-gather.6.cloned.1.call-done = bf16[2,12288,1,128]{3,1,2,0:T(8,128)(2,1)} async-done(((bf16[2,384,1,128]{3,1,2,0:T(8,128)(2,1)}), bf16[2,12288,1,128]{3,1,2,0:T(8,128)(2,1)}) %all-gather.6.cloned.1.call-update) | async-done | bytes 6291472 | tf_op jit(solution)/shard_map/all_gather | solution.py:218
  121.4 130.8 %while.19 = (s32[]{:T(128)}, f32[384,1,128]{0,2,1:T(8,128)S(1)}, f32[384,1]{0,1:T(1,128)S(1)}, s32[]{:T(128)}, bf16[2,12288,1,128]{3,1,2,0:T(8,128)(2,1)}, /*ind...) while((s32[]{:T(128)}, f32[384,1,128]{0,2,1:T(8,128)S(1)}, ...), condition=%wide.region_11.12_spmd.clone, body=%wide.region_4.11_spmd.clone.sunk | while | flops 786794880 | bytes 14367049 | solution.py:227
  121.4 16.3 %conditional.3 = ((f32[384,1,128]{0,2,1:T(8,128)S(1)}, f32[384,1]{0,1:T(1,128)S(1)})) conditional(s32[]{:T(128)} %convert_element_type.431, (f32[384,1,128]{0,2,1:T(8,128)S(1)}, f32[384,1]{0,1:T(1,128)S(1)}) %tuple.82, (s32[]{:T(128)}, s32[]{:T(128)}, bf16[2,12288,1,128]{3,1,2,0:T(8,128)(2,1)}, bf16[384,1,128]{2,0,1:T(8,128)(2,1)S(1)}, f32[1]{0:T(128)}, ...), branch_computations={%region_5.5_spmd, %region_6.10_spmd} | conditional | flops 786794880 | bytes 14365306 | solution.py:225
  121.5 4.5 %fusion.11 = (f32[384]{0:T(512)S(1)}, f32[1536,384]{1,0:T(8,128)S(1)}) fusion(s32[384]{0:T(512)S(1)} %broadcast_add_fusion, s32[1536]{0:T(1024)S(1)} %add.223, pred[1536]{0:T(1024)(128)(4,1)S(1)} %broadcast_compare_fusion, f32[]{:T(128)} %bitcast.2, bf16[384,1,128]{2,0,1:T(8,128)(2,1)S(1)} %get-tuple-element.360, ...), kind=kOutput, calls=%fused_computation.14 | convolution fusion | flops 159841920 | bytes 2862084 | tf_op jit(solution)/shard_map/while/body/eval_jaxpr/cond/branch_1_fun/thd,shd->hts/dot_general | solution.py:133
  131.1 6.5 %fusion.33 = f32[384,128]{0,1:T(8,128)S(1)} fusion(bf16[4,384,128]{2,1,0:T(8,128)(2,1)S(1)} %bitcast.199, f32[384,4,384]{2,0,1:T(8,128)} %copy.21, s32[4,384]{1,0:T(4,128)S(1)} %add_add_fusion, s32[384]{0:T(512)S(1)} %broadcast_add_fusion, pred[4,384]{1,0:T(4,128)(4,1)S(1)} %broadcast_compare_fusion.1, f32[384,4]{0,1:T(4,128)S(1)} %add_exponential_fusion), kind=kOutput, calls=%fused_computation.31 | convolution fusion | flops 619216896 | bytes 2964480 | tf_op jit(solution)/shard_map/while/body/eval_jaxpr/cond/branch_1_fun/htgs,gshe->thge/dot_general | solution.py:145
  137.8 16.3 %conditional.3 = ((f32[384,1,128]{0,2,1:T(8,128)S(1)}, f32[384,1]{0,1:T(1,128)S(1)})) conditional(s32[]{:T(128)} %convert_element_type.431, (f32[384,1,128]{0,2,1:T(8,128)S(1)}, f32[384,1]{0,1:T(1,128)S(1)}) %tuple.82, (s32[]{:T(128)}, s32[]{:T(128)}, bf16[2,12288,1,128]{3,1,2,0:T(8,128)(2,1)}, bf16[384,1,128]{2,0,1:T(8,128)(2,1)S(1)}, f32[1]{0:T(128)}, ...), branch_computations={%region_5.5_spmd, %region_6.10_spmd} | conditional | flops 786794880 | bytes 14365306 | solution.py:225
  137.8 4.5 %fusion.11 = (f32[384]{0:T(512)S(1)}, f32[1536,384]{1,0:T(8,128)S(1)}) fusion(s32[384]{0:T(512)S(1)} %broadcast_add_fusion, s32[1536]{0:T(1024)S(1)} %add.223, pred[1536]{0:T(1024)(128)(4,1)S(1)} %broadcast_compare_fusion, f32[]{:T(128)} %bitcast.2, bf16[384,1,128]{2,0,1:T(8,128)(2,1)S(1)} %get-tuple-element.360, ...), kind=kOutput, calls=%fused_computation.14 | convolution fusion | flops 159841920 | bytes 2862084 | tf_op jit(solution)/shard_map/while/body/eval_jaxpr/cond/branch_1_fun/thd,shd->hts/dot_general | solution.py:133
  147.5 6.5 %fusion.33 = f32[384,128]{0,1:T(8,128)S(1)} fusion(bf16[4,384,128]{2,1,0:T(8,128)(2,1)S(1)} %bitcast.199, f32[384,4,384]{2,0,1:T(8,128)} %copy.21, s32[4,384]{1,0:T(4,128)S(1)} %add_add_fusion, s32[384]{0:T(512)S(1)} %broadcast_add_fusion, pred[4,384]{1,0:T(4,128)(4,1)S(1)} %broadcast_compare_fusion.1, f32[384,4]{0,1:T(4,128)S(1)} %add_exponential_fusion), kind=kOutput, calls=%fused_computation.31 | convolution fusion | flops 619216896 | bytes 2964480 | tf_op jit(solution)/shard_map/while/body/eval_jaxpr/cond/branch_1_fun/htgs,gshe->thge/dot_general | solution.py:145
  154.1 16.3 %conditional.3 = ((f32[384,1,128]{0,2,1:T(8,128)S(1)}, f32[384,1]{0,1:T(1,128)S(1)})) conditional(s32[]{:T(128)} %convert_element_type.431, (f32[384,1,128]{0,2,1:T(8,128)S(1)}, f32[384,1]{0,1:T(1,128)S(1)}) %tuple.82, (s32[]{:T(128)}, s32[]{:T(128)}, bf16[2,12288,1,128]{3,1,2,0:T(8,128)(2,1)}, bf16[384,1,128]{2,0,1:T(8,128)(2,1)S(1)}, f32[1]{0:T(128)}, ...), branch_computations={%region_5.5_spmd, %region_6.10_spmd} | conditional | flops 786794880 | bytes 14365306 | solution.py:225
  154.2 4.5 %fusion.11 = (f32[384]{0:T(512)S(1)}, f32[1536,384]{1,0:T(8,128)S(1)}) fusion(s32[384]{0:T(512)S(1)} %broadcast_add_fusion, s32[1536]{0:T(1024)S(1)} %add.223, pred[1536]{0:T(1024)(128)(4,1)S(1)} %broadcast_compare_fusion, f32[]{:T(128)} %bitcast.2, bf16[384,1,128]{2,0,1:T(8,128)(2,1)S(1)} %get-tuple-element.360, ...), kind=kOutput, calls=%fused_computation.14 | convolution fusion | flops 159841920 | bytes 2862084 | tf_op jit(solution)/shard_map/while/body/eval_jaxpr/cond/branch_1_fun/thd,shd->hts/dot_general | solution.py:133
  163.8 6.5 %fusion.33 = f32[384,128]{0,1:T(8,128)S(1)} fusion(bf16[4,384,128]{2,1,0:T(8,128)(2,1)S(1)} %bitcast.199, f32[384,4,384]{2,0,1:T(8,128)} %copy.21, s32[4,384]{1,0:T(4,128)S(1)} %add_add_fusion, s32[384]{0:T(512)S(1)} %broadcast_add_fusion, pred[4,384]{1,0:T(4,128)(4,1)S(1)} %broadcast_compare_fusion.1, f32[384,4]{0,1:T(4,128)S(1)} %add_exponential_fusion), kind=kOutput, calls=%fused_computation.31 | convolution fusion | flops 619216896 | bytes 2964480 | tf_op jit(solution)/shard_map/while/body/eval_jaxpr/cond/branch_1_fun/htgs,gshe->thge/dot_general | solution.py:145
  170.5 16.3 %conditional.3 = ((f32[384,1,128]{0,2,1:T(8,128)S(1)}, f32[384,1]{0,1:T(1,128)S(1)})) conditional(s32[]{:T(128)} %convert_element_type.431, (f32[384,1,128]{0,2,1:T(8,128)S(1)}, f32[384,1]{0,1:T(1,128)S(1)}) %tuple.82, (s32[]{:T(128)}, s32[]{:T(128)}, bf16[2,12288,1,128]{3,1,2,0:T(8,128)(2,1)}, bf16[384,1,128]{2,0,1:T(8,128)(2,1)S(1)}, f32[1]{0:T(128)}, ...), branch_computations={%region_5.5_spmd, %region_6.10_spmd} | conditional | flops 786794880 | bytes 14365306 | solution.py:225
  170.5 4.5 %fusion.11 = (f32[384]{0:T(512)S(1)}, f32[1536,384]{1,0:T(8,128)S(1)}) fusion(s32[384]{0:T(512)S(1)} %broadcast_add_fusion, s32[1536]{0:T(1024)S(1)} %add.223, pred[1536]{0:T(1024)(128)(4,1)S(1)} %broadcast_compare_fusion, f32[]{:T(128)} %bitcast.2, bf16[384,1,128]{2,0,1:T(8,128)(2,1)S(1)} %get-tuple-element.360, ...), kind=kOutput, calls=%fused_computation.14 | convolution fusion | flops 159841920 | bytes 2862084 | tf_op jit(solution)/shard_map/while/body/eval_jaxpr/cond/branch_1_fun/thd,shd->hts/dot_general | solution.py:133
  180.2 6.5 %fusion.33 = f32[384,128]{0,1:T(8,128)S(1)} fusion(bf16[4,384,128]{2,1,0:T(8,128)(2,1)S(1)} %bitcast.199, f32[384,4,384]{2,0,1:T(8,128)} %copy.21, s32[4,384]{1,0:T(4,128)S(1)} %add_add_fusion, s32[384]{0:T(512)S(1)} %broadcast_add_fusion, pred[4,384]{1,0:T(4,128)(4,1)S(1)} %broadcast_compare_fusion.1, f32[384,4]{0,1:T(4,128)S(1)} %add_exponential_fusion), kind=kOutput, calls=%fused_computation.31 | convolution fusion | flops 619216896 | bytes 2964480 | tf_op jit(solution)/shard_map/while/body/eval_jaxpr/cond/branch_1_fun/htgs,gshe->thge/dot_general | solution.py:145
  186.8 16.3 %conditional.3 = ((f32[384,1,128]{0,2,1:T(8,128)S(1)}, f32[384,1]{0,1:T(1,128)S(1)})) conditional(s32[]{:T(128)} %convert_element_type.431, (f32[384,1,128]{0,2,1:T(8,128)S(1)}, f32[384,1]{0,1:T(1,128)S(1)}) %tuple.82, (s32[]{:T(128)}, s32[]{:T(128)}, bf16[2,12288,1,128]{3,1,2,0:T(8,128)(2,1)}, bf16[384,1,128]{2,0,1:T(8,128)(2,1)S(1)}, f32[1]{0:T(128)}, ...), branch_computations={%region_5.5_spmd, %region_6.10_spmd} | conditional | flops 786794880 | bytes 14365306 | solution.py:225
  186.9 4.5 %fusion.11 = (f32[384]{0:T(512)S(1)}, f32[1536,384]{1,0:T(8,128)S(1)}) fusion(s32[384]{0:T(512)S(1)} %broadcast_add_fusion, s32[1536]{0:T(1024)S(1)} %add.223, pred[1536]{0:T(1024)(128)(4,1)S(1)} %broadcast_compare_fusion, f32[]{:T(128)} %bitcast.2, bf16[384,1,128]{2,0,1:T(8,128)(2,1)S(1)} %get-tuple-element.360, ...), kind=kOutput, calls=%fused_computation.14 | convolution fusion | flops 159841920 | bytes 2862084 | tf_op jit(solution)/shard_map/while/body/eval_jaxpr/cond/branch_1_fun/thd,shd->hts/dot_general | solution.py:133
  196.5 6.5 %fusion.33 = f32[384,128]{0,1:T(8,128)S(1)} fusion(bf16[4,384,128]{2,1,0:T(8,128)(2,1)S(1)} %bitcast.199, f32[384,4,384]{2,0,1:T(8,128)} %copy.21, s32[4,384]{1,0:T(4,128)S(1)} %add_add_fusion, s32[384]{0:T(512)S(1)} %broadcast_add_fusion, pred[4,384]{1,0:T(4,128)(4,1)S(1)} %broadcast_compare_fusion.1, f32[384,4]{0,1:T(4,128)S(1)} %add_exponential_fusion), kind=kOutput, calls=%fused_computation.31 | convolution fusion | flops 619216896 | bytes 2964480 | tf_op jit(solution)/shard_map/while/body/eval_jaxpr/cond/branch_1_fun/htgs,gshe->thge/dot_general | solution.py:145
  203.2 16.3 %conditional.3 = ((f32[384,1,128]{0,2,1:T(8,128)S(1)}, f32[384,1]{0,1:T(1,128)S(1)})) conditional(s32[]{:T(128)} %convert_element_type.431, (f32[384,1,128]{0,2,1:T(8,128)S(1)}, f32[384,1]{0,1:T(1,128)S(1)}) %tuple.82, (s32[]{:T(128)}, s32[]{:T(128)}, bf16[2,12288,1,128]{3,1,2,0:T(8,128)(2,1)}, bf16[384,1,128]{2,0,1:T(8,128)(2,1)S(1)}, f32[1]{0:T(128)}, ...), branch_computations={%region_5.5_spmd, %region_6.10_spmd} | conditional | flops 786794880 | bytes 14365306 | solution.py:225
  203.3 4.5 %fusion.11 = (f32[384]{0:T(512)S(1)}, f32[1536,384]{1,0:T(8,128)S(1)}) fusion(s32[384]{0:T(512)S(1)} %broadcast_add_fusion, s32[1536]{0:T(1024)S(1)} %add.223, pred[1536]{0:T(1024)(128)(4,1)S(1)} %broadcast_compare_fusion, f32[]{:T(128)} %bitcast.2, bf16[384,1,128]{2,0,1:T(8,128)(2,1)S(1)} %get-tuple-element.360, ...), kind=kOutput, calls=%fused_computation.14 | convolution fusion | flops 159841920 | bytes 2862084 | tf_op jit(solution)/shard_map/while/body/eval_jaxpr/cond/branch_1_fun/thd,shd->hts/dot_general | solution.py:133
  212.9 6.5 %fusion.33 = f32[384,128]{0,1:T(8,128)S(1)} fusion(bf16[4,384,128]{2,1,0:T(8,128)(2,1)S(1)} %bitcast.199, f32[384,4,384]{2,0,1:T(8,128)} %copy.21, s32[4,384]{1,0:T(4,128)S(1)} %add_add_fusion, s32[384]{0:T(512)S(1)} %broadcast_add_fusion, pred[4,384]{1,0:T(4,128)(4,1)S(1)} %broadcast_compare_fusion.1, f32[384,4]{0,1:T(4,128)S(1)} %add_exponential_fusion), kind=kOutput, calls=%fused_computation.31 | convolution fusion | flops 619216896 | bytes 2964480 | tf_op jit(solution)/shard_map/while/body/eval_jaxpr/cond/branch_1_fun/htgs,gshe->thge/dot_general | solution.py:145
  219.5 16.3 %conditional.3 = ((f32[384,1,128]{0,2,1:T(8,128)S(1)}, f32[384,1]{0,1:T(1,128)S(1)})) conditional(s32[]{:T(128)} %convert_element_type.431, (f32[384,1,128]{0,2,1:T(8,128)S(1)}, f32[384,1]{0,1:T(1,128)S(1)}) %tuple.82, (s32[]{:T(128)}, s32[]{:T(128)}, bf16[2,12288,1,128]{3,1,2,0:T(8,128)(2,1)}, bf16[384,1,128]{2,0,1:T(8,128)(2,1)S(1)}, f32[1]{0:T(128)}, ...), branch_computations={%region_5.5_spmd, %region_6.10_spmd} | conditional | flops 786794880 | bytes 14365306 | solution.py:225
  219.6 4.5 %fusion.11 = (f32[384]{0:T(512)S(1)}, f32[1536,384]{1,0:T(8,128)S(1)}) fusion(s32[384]{0:T(512)S(1)} %broadcast_add_fusion, s32[1536]{0:T(1024)S(1)} %add.223, pred[1536]{0:T(1024)(128)(4,1)S(1)} %broadcast_compare_fusion, f32[]{:T(128)} %bitcast.2, bf16[384,1,128]{2,0,1:T(8,128)(2,1)S(1)} %get-tuple-element.360, ...), kind=kOutput, calls=%fused_computation.14 | convolution fusion | flops 159841920 | bytes 2862084 | tf_op jit(solution)/shard_map/while/body/eval_jaxpr/cond/branch_1_fun/thd,shd->hts/dot_general | solution.py:133
  229.2 6.5 %fusion.33 = f32[384,128]{0,1:T(8,128)S(1)} fusion(bf16[4,384,128]{2,1,0:T(8,128)(2,1)S(1)} %bitcast.199, f32[384,4,384]{2,0,1:T(8,128)} %copy.21, s32[4,384]{1,0:T(4,128)S(1)} %add_add_fusion, s32[384]{0:T(512)S(1)} %broadcast_add_fusion, pred[4,384]{1,0:T(4,128)(4,1)S(1)} %broadcast_compare_fusion.1, f32[384,4]{0,1:T(4,128)S(1)} %add_exponential_fusion), kind=kOutput, calls=%fused_computation.31 | convolution fusion | flops 619216896 | bytes 2964480 | tf_op jit(solution)/shard_map/while/body/eval_jaxpr/cond/branch_1_fun/htgs,gshe->thge/dot_general | solution.py:145
  235.9 16.3 %conditional.3 = ((f32[384,1,128]{0,2,1:T(8,128)S(1)}, f32[384,1]{0,1:T(1,128)S(1)})) conditional(s32[]{:T(128)} %convert_element_type.431, (f32[384,1,128]{0,2,1:T(8,128)S(1)}, f32[384,1]{0,1:T(1,128)S(1)}) %tuple.82, (s32[]{:T(128)}, s32[]{:T(128)}, bf16[2,12288,1,128]{3,1,2,0:T(8,128)(2,1)}, bf16[384,1,128]{2,0,1:T(8,128)(2,1)S(1)}, f32[1]{0:T(128)}, ...), branch_computations={%region_5.5_spmd, %region_6.10_spmd} | conditional | flops 786794880 | bytes 14365306 | solution.py:225
  236.0 4.5 %fusion.11 = (f32[384]{0:T(512)S(1)}, f32[1536,384]{1,0:T(8,128)S(1)}) fusion(s32[384]{0:T(512)S(1)} %broadcast_add_fusion, s32[1536]{0:T(1024)S(1)} %add.223, pred[1536]{0:T(1024)(128)(4,1)S(1)} %broadcast_compare_fusion, f32[]{:T(128)} %bitcast.2, bf16[384,1,128]{2,0,1:T(8,128)(2,1)S(1)} %get-tuple-element.360, ...), kind=kOutput, calls=%fused_computation.14 | convolution fusion | flops 159841920 | bytes 2862084 | tf_op jit(solution)/shard_map/while/body/eval_jaxpr/cond/branch_1_fun/thd,shd->hts/dot_general | solution.py:133
  245.6 6.5 %fusion.33 = f32[384,128]{0,1:T(8,128)S(1)} fusion(bf16[4,384,128]{2,1,0:T(8,128)(2,1)S(1)} %bitcast.199, f32[384,4,384]{2,0,1:T(8,128)} %copy.21, s32[4,384]{1,0:T(4,128)S(1)} %add_add_fusion, s32[384]{0:T(512)S(1)} %broadcast_add_fusion, pred[4,384]{1,0:T(4,128)(4,1)S(1)} %broadcast_compare_fusion.1, f32[384,4]{0,1:T(4,128)S(1)} %add_exponential_fusion), kind=kOutput, calls=%fused_computation.31 | convolution fusion | flops 619216896 | bytes 2964480 | tf_op jit(solution)/shard_map/while/body/eval_jaxpr/cond/branch_1_fun/htgs,gshe->thge/dot_general | solution.py:145
  252.6 2.7 add_convert_fusion
  255.4 25.7 %all_to_all.11 = bf16[8,256,384]{1,2,0:T(8,128)(2,1)S(1)} all-to-all(bf16[8,256,384]{1,2,0:T(8,128)(2,1)S(1)} %bitcast.200), channel_id=1, replica_groups=mesh['sp_0'=8,'sp_1'=4,'tp'=8] {'tp'}, dimensions={0} | all-to-all | bytes 3145728 | tf_op jit(solution)/shard_map/all_to_all | solution.py:84
  (172 shorter events, 55.1 us)
Async XLA Ops:
  6.5 86.4 %copy-start = (bf16[128,2048]{1,0:T(8,128)(2,1)S(1)}, bf16[128,2048]{1,0:T(8,128)(2,1)}, u32[]{:S(2)}) copy-start(bf16[128,2048]{1,0:T(8,128)(2,1)} %param.24) | copy-start | bytes 1572868
  6.5 114.8 %all-gather.6.cloned.1.call-start = ((), (), s32[]{:S(2)}) async-start(), calls=%async_computation.2 | async-start | bytes 6488064 | tf_op jit(solution)/shard_map/all_gather | solution.py:218
  7.7 26.2 %copy-start.1 = (bf16[2048,128]{1,0:T(8,128)(2,1)S(1)}, bf16[2048,128]{1,0:T(8,128)(2,1)}, u32[]{:S(2)}) copy-start(bf16[2048,128]{1,0:T(8,128)(2,1)} %param.20) | copy-start | bytes 1572868
  7.8 26.6 %copy-start.2 = (bf16[2048,128]{1,0:T(8,128)(2,1)S(1)}, bf16[2048,128]{1,0:T(8,128)(2,1)}, u32[]{:S(2)}) copy-start(bf16[2048,128]{1,0:T(8,128)(2,1)} %param.21) | copy-start | bytes 1572868
  34.5 1.4 copy-start.5
  34.5 4.9 %copy-start.6 = (bf16[2048,128]{1,0:T(8,128)(2,1)S(1)}, bf16[2048,128]{1,0:T(8,128)(2,1)}, u32[]{:S(2)}) copy-start(bf16[2048,128]{1,0:T(8,128)(2,1)} %param.16) | copy-start | bytes 1572868
  35.2 4.7 %copy-start.7 = (bf16[2048,128]{1,0:T(8,128)(2,1)S(1)}, bf16[2048,128]{1,0:T(8,128)(2,1)}, u32[]{:S(2)}) copy-start(bf16[2048,128]{1,0:T(8,128)(2,1)} %param.17) | copy-start | bytes 1572868
  39.9 1.0 copy-start.3
  41.6 50.7 %copy-start.4 = (bf16[2048,128]{1,0:T(8,128)(2,1)S(1)}, bf16[2048,128]{1,0:T(8,128)(2,1)}, u32[]{:S(2)}) copy-start(bf16[2048,128]{1,0:T(8,128)(2,1)} %param.19) | copy-start | bytes 1572868
Sparse Core Ops, SparseCore 0:
  36.0 85.2 all-gather.5
where the time goes:
time: 290 us; the launch traced here: 289 us
  matrix products  99.3 us (34%)
  blocking collectives  89.4 us (31%)
  local copies, waits for them, and re-layouts  28.4 us (10%)
  waiting for transfers between devices  26.2 us (9%)
  between operations  24 us (8%)
  other arithmetic  20.6 us (7%)
    dot_general x8, matrix products, stick_group(): jnp.einsum('htgs,gshe->thge', weights, value_groups, preferred_element_ty...  52.3 us
    all_gather x2, blocking collectives, gathered_once(): both, at, found = (lax.all_gather(jnp.concatenate(lines), axis), 0, {})  37.7 us
    dot_general x8, matrix products, stick_group(): jnp.einsum('thd,shd->hts', queries, key_pairs[0], preferred_element_type=...  36 us
    all_gather x1, waiting for transfers between devices, body(): every_pair = lax.all_gather(stick_pairs, SP, axis=1, tiled=True)  26.1 us
    all_to_all x1, blocking collectives, from_everyone(): lax.all_to_all(jnp.broadcast_to(array[None], (size, *array.shape)), axis,...  26 us
    all_to_all x1, blocking collectives, sent_and_summed(): lax.all_to_all(pieces, axis, split_axis=0, concat_axis=0, tiled=True)  25.7 us
    reduce_sum x8, other arithmetic, stick_group(): totals = jnp.transpose(jnp.sum(failure, axis=3), (1, 0, 2))  16.4 us
    reshape x8, local copies, waits for them, and re-layouts, stick_group(): logits = logits.reshape(head_count, -1, shard_count, shard_rows)  15.7 us
  transfers between devices with their start and end apart: 1, of which 1 were waited for; matrix products, arithmetic and copies ran while one was open for 4% of the time, Pallas kernels for 0%

commit v1 on v0

v1 whole, which is shorter than its diff:
```python
import math

import jax
import jax.numpy as jnp
import numpy as np
from jax import lax
from jax.experimental import pallas as pl
from jax.experimental.pallas import tpu as pltpu
from jax.sharding import Mesh
from jax.sharding import PartitionSpec as P

HEAD_DIM = 128
ROWS = 384
HALF = ROWS // 2
D = 2048
NZ, NX, NY, NC = 8, 4, 4, 2
SP = ("z", "x")
TP = ("y", "c")
EPS = 1e-05
ROPE_BASE = 10000.0
LOG2E = math.log2(math.e)
SCALE = HEAD_DIM**-0.5
CLAMP = 120.0
MESH = pl.DeviceIdType.MESH
F32, BF16 = jnp.float32, jnp.bfloat16


def angle_tables():
    half = HEAD_DIM // 2
    inverse = ROPE_BASE ** (-np.arange(half, dtype=np.float64) / half)
    sign = np.concatenate([-np.ones(half), np.ones(half)])
    inside = np.arange(ROWS)[:, None] * np.concatenate([inverse, inverse])[None]
    start = (np.arange(NZ * NX) * ROWS)[:, None] * np.concatenate([inverse, inverse])[None]
    return tuple(
        np.asarray(t, np.float32)
        for t in (np.cos(inside), np.sin(inside) * sign, np.cos(start), np.sin(start) * sign)
    )


def head_norm(values):
    centred = values - jnp.mean(values, axis=-1, keepdims=True)
    spread = jnp.mean(centred * centred, axis=-1, keepdims=True)
    return centred * lax.rsqrt(spread + EPS)


def dot(a, b):
    return jnp.dot(a, b, preferred_element_type=F32)


def dot_t(a, b):
    return lax.dot_general(a, b, (((1,), (1,)), ((), ())), preferred_element_type=F32)


def remote(src, dst, ssem, rsem, device):
    return pltpu.make_async_remote_copy(
        src_ref=src,
        dst_ref=dst,
        send_sem=ssem,
        recv_sem=rsem,
        device_id=device,
        device_id_type=MESH,
    )


class Ring:
    def __init__(self, axis, me, view, ssem, rsem):
        self.axis, self.me, self.view, self.ssem, self.rsem = axis, me, view, ssem, rsem
        self.nxt, self.prv, self.far = (me + 1) % 4, (me + 3) % 4, (me + 2) % 4

    def copy(self, slot, half, index, to):
        ref = self.view(slot, half)
        return remote(ref, ref, self.ssem.at[index], self.rsem.at[index], {self.axis: to})

    def sends(self):
        me, n, p = self.me, self.nxt, self.prv
        return [
            self.copy(me, 0, 0, n),
            self.copy(me, 1, 3, p),
            self.copy(me, 1, 1, n),
            self.copy(me, 0, 2, p),
        ]

    def start(self):
        for c in self.sends():
            c.start()

    def landed(self, index):
        slot = (self.prv, self.prv, self.nxt, self.nxt, self.far, self.far)[index]
        return self.copy(slot, index % 2, index, self.nxt)

    def wait(self, index):
        self.landed(index).wait_recv()

    def onward(self, index):
        if index == 0:
            return self.copy(self.prv, 0, 4, self.nxt)
        return self.copy(self.nxt, 1, 5, self.prv)

    def drain(self):
        for c in self.sends() + [self.onward(0), self.onward(3)]:
            c.wait_send()


class PairRing(Ring):
    def __init__(self, y, c, view, ssem, rsem, psem, qsem):
        super().__init__("y", y, lambda s, h: view(s, h, c), ssem, rsem)
        self.c, self.view2, self.psem, self.qsem = c, view, psem, qsem

    def across(self, index, core):
        slot = (self.prv, self.prv, self.nxt, self.nxt, self.far, self.far, self.me, self.me)[index]
        ref = self.view2(slot, index % 2, core)
        return remote(ref, ref, self.psem.at[index], self.qsem.at[index], {"c": 1 - self.c})

    def begin(self):
        self.start()
        self.across(6, self.c).start()
        self.across(7, self.c).start()

    def pump(self, index):
        self.wait(index)
        if index in (0, 3):
            self.onward(index).start()
        self.across(index, self.c).start()

    def other(self, index):
        self.across(index, 1 - self.c).wait_recv()

    def finish(self):
        self.drain()
        for i in range(8):
            self.across(i, self.c).wait_send()


def exchange(axis, me, count, src, slot, ssem, rsem):
    out = []
    for i in range(1, count):
        out.append(
            remote(src, slot(me, i), ssem.at[i - 1], rsem.at[i - 1], {axis: (me + i) % count})
        )
    return out


def kernel(
    tokens,
    decays,
    bias,
    base_cos,
    base_sin,
    w0,
    w1,
    w2,
    w3,
    w4,
    w5,
    o0,
    o1,
    tab_cos,
    tab_sin,
    out,
    tok,
    wbuf,
    owbuf,
    owr,
    ows,
    tabs,
    acc,
    qall,
    kbuf,
    vbuf,
    part,
    tots,
    ttx,
    csend,
    crecv,
    fresh,
    dec,
    smsg,
    stq,
    rbuf,
    sbuf,
    rq,
    rk,
    rv,
    cums,
    local,
    tri12,
    tri0,
    lsem,
    tok_s,
    tok_r,
    ret_s,
    ret_r,
    stk_s,
    stk_r,
    q_s,
    q_r,
    z_s,
    z_r,
    x_s,
    x_r,
    s_s,
    s_r,
    ow_s,
    ow_r,
):
    z, x, y, c = (lax.axis_index(a) for a in ("z", "x", "y", "c"))
    barrier = pltpu.get_barrier_semaphore()
    peers = [{"z": (z + i) % NZ} for i in range(1, NZ)]
    peers += [{"x": (x + i) % NX} for i in range(1, NX)]
    peers += [{"c": 1 - c}]
    for i in range(1, NY):
        peers += [{"y": (y + i) % NY}, {"y": (y + i) % NY, "c": 1 - c}]
    for peer in peers:
        pl.semaphore_signal(barrier, inc=1, device_id=peer, device_id_type=MESH)

    loads = [
        pltpu.make_async_copy(w, wbuf.at[:, pl.ds(128 * i, 128)], lsem.at[i])
        for i, w in enumerate((w0, w1, w2, w3, w4, w5))
    ]
    late = [
        pltpu.make_async_copy(tab_cos, tabs.at[0], lsem.at[6]),
        pltpu.make_async_copy(tab_sin, tabs.at[1], lsem.at[7]),
        pltpu.make_async_copy(o0, owbuf.at[pl.ds(0, 128)], lsem.at[8]),
        pltpu.make_async_copy(o1, owbuf.at[pl.ds(128, 128)], lsem.at[9]),
    ]
    own_tok = pltpu.make_async_copy(
        tokens, tok.at[y, :, pl.ds(pl.multiple_of(c * 256, 256), 256)], lsem.at[10]
    )
    own_tok.start()
    for load in loads + late:
        load.start()
    own_tok.wait()
    pl.semaphore_wait(barrier, len(peers))

    def tok_view(slot, half, core):
        lanes = pl.ds(pl.multiple_of(core * 256, 256), 256)
        return tok.at[slot, pl.ds(HALF * half, HALF), lanes]

    ring = PairRing(y, c, tok_view, tok_s.at[0], tok_r.at[0], tok_s.at[1], tok_r.at[1])
    ring.begin()

    i0 = lax.broadcasted_iota(jnp.int32, (256, 384), 0)
    i1 = lax.broadcasted_iota(jnp.int32, (256, 384), 1)
    tri12[...] = ((i0 > i1) | (i1 >= 256)).astype(BF16)
    j0 = lax.broadcasted_iota(jnp.int32, (128, 256), 0)
    j1 = lax.broadcasted_iota(jnp.int32, (128, 256), 1)
    tri0[...] = ((j0 > j1) | (j1 >= 128)).astype(BF16)
    r0 = lax.broadcasted_iota(jnp.int32, (ROWS, ROWS), 0)
    r1 = lax.broadcasted_iota(jnp.int32, (ROWS, ROWS), 1)
    lower = (r0 >= r1).astype(BF16)
    wide = jnp.broadcast_to(decays[...], (ROWS, HEAD_DIM))
    hi = wide.astype(BF16)
    rest = wide - hi.astype(F32)
    mid = rest.astype(BF16)
    low = (rest - mid.astype(F32)).astype(BF16)
    cum = dot(lower, hi) + dot(lower, mid) + dot(lower, low)
    cums[...] = cum
    dec[x] = jnp.broadcast_to(cum[ROWS - 1 :, :], (8, HEAD_DIM))
    dec_out = exchange("x", x, NX, dec.at[x], lambda me, i: dec.at[me], x_s.at[0], x_r.at[0])
    for copy in dec_out:
        copy.start()

    ring.pump(0)
    ring.pump(3)
    ring.pump(1)
    ring.pump(2)
    for load in loads:
        load.wait()
    ring.other(6)
    ring.other(7)

    def project(slot):
        rows = pl.ds(pl.multiple_of(slot * 512, 512), 512)
        return dot(tok[slot], wbuf[rows, :])

    acc[...] = project(y)
    ring.pump(4)
    ring.pump(5)
    ring.other(0)
    ring.other(1)
    acc[...] += project(ring.prv)
    ring.other(2)
    ring.other(3)
    acc[...] += project(ring.nxt)
    ring.other(4)
    ring.other(5)
    acc[...] += project(ring.far)
    total = acc[...]
    qall[x] = total[:, 384:512].astype(BF16)
    kbuf[0] = total[:, 512:640].astype(BF16)
    vbuf[0] = total[:, 640:768].astype(BF16)

    zu, zd = (z + 1) % NZ, (z + NZ - 1) % NZ

    def hop(buf, which, frm, to, device):
        return remote(
            buf.at[frm], buf.at[to], z_s.at[which, to], z_r.at[which, to], {"z": device}
        )

    def up(buf, which, d):
        return hop(buf, which, d, d + 1, zu)

    def down(buf, which, d):
        return hop(buf, which, d, d - 1, zd)

    def here(buf, which, d):
        hop(buf, which, d, d, zu).wait_recv()

    up(kbuf, 0, 0).start()
    hop(kbuf, 0, 0, 7, zd).start()
    qring = Ring(
        "x", x, lambda s, h: qall.at[s, pl.ds(HALF * h, HALF)], q_s, q_r
    )
    qring.start()
    up(vbuf, 1, 0).start()
    hop(vbuf, 1, 0, 7, zd).start()
    ring.finish()

    for load in late:
        load.wait()
    sp = z * NX + x
    bc, bs = base_cos[pl.ds(sp, 1), :], base_sin[pl.ds(sp, 1), :]
    cosine = tabs[0] * bc - tabs[1] * bs
    sine = tabs[1] * bc + tabs[0] * bs

    def rotate(values):
        return values * cosine + pltpu.roll(values, HEAD_DIM // 2, 1) * sine

    qr = rotate(acc[:, 0:128].astype(BF16).astype(F32)).astype(BF16)
    kr = (rotate(acc[:, 128:256].astype(BF16).astype(F32)) * SCALE).astype(BF16)
    vr = acc[:, 256:384].astype(BF16)
    rq[...] = qr
    cum = cums[...]
    weighted = (kr.astype(F32) * jnp.exp(cum[ROWS - 1 :, :] - cum)).astype(BF16)
    rk[...] = kr
    rv[...] = vr
    fresh[x] = lax.dot_general(
        weighted, vr, (((0,), (0,)), ((), ())), preferred_element_type=F32
    ).astype(BF16)
    fresh_out = exchange(
        "x", x, NX, fresh.at[x], lambda me, i: fresh.at[me], x_s.at[1], x_r.at[1]
    )
    for copy in fresh_out:
        copy.start()

    def weight_copies():
        copies = []
        for i in range(NY):
            for other in range(2):
                if i == 0 and other == 0:
                    continue
                ty, tc = (y + i) % NY, (c + other) % 2
                columns = pl.ds(pl.multiple_of((ty * 2 + tc) * 256, 256), 256)
                rows = pl.ds(pl.multiple_of(c * 128, 128), 128)
                for m, dst in enumerate((owr, ows)):
                    copies.append(
                        remote(
                            owbuf.at[pl.ds(128 * m, 128), columns],
                            dst.at[y, rows],
                            ow_s.at[m, i, other],
                            ow_r.at[m, i, other],
                            {"y": ty, "c": tc},
                        )
                    )
        return copies

    own_rows = pl.ds(pl.multiple_of(c * 128, 128), 128)
    own_columns = pl.ds(pl.multiple_of((y * 2 + c) * 256, 256), 256)
    keep = [
        pltpu.make_async_copy(owbuf.at[pl.ds(128 * m, 128), own_columns], dst.at[y, own_rows], lsem.at[11 + m])
        for m, dst in enumerate((owr, ows))
    ]
    for copy in weight_copies() + keep:
        copy.start()

    tots[...] = jnp.zeros_like(tots)
    offset = bias[0] * LOG2E
    lanes = lax.broadcasted_iota(jnp.int32, (ROWS, HEAD_DIM), 1)

    def pair(d, xq, masked):
        scores = dot_t(qall[xq], kbuf[d])
        u = scores * (SCALE * LOG2E) + offset
        soft = jnp.maximum(jnp.log2(1.0 + jnp.exp2(jnp.minimum(u, CLAMP))), u)
        if masked:
            visible = lax.broadcasted_iota(jnp.int32, (ROWS, ROWS), 0) > (
                lax.broadcasted_iota(jnp.int32, (ROWS, ROWS), 1)
            )
            success = u - soft
            soft = jnp.where(visible, soft, 0.0)
        else:
            success = u - soft
        f = soft.astype(BF16)
        r12 = dot(f[:, 128:], tri12[...])
        rr = dot(f[:, :128], tri0[...])
        later = r12[:, 256:]
        suffix = jnp.concatenate([rr[:, :128] + later, r12[:, :256]], axis=1)
        weights = jnp.exp2(success - suffix)
        if masked:
            weights = jnp.where(visible, weights, 0.0)
        part[d, xq] = dot(weights.astype(BF16), vbuf[d])
        tots[xq] = jnp.where(lanes == d, rr[:, 128:] + later, tots[xq])

    def pairs(d):
        @pl.loop(0, NX)
        def _(xq):
            run = jnp.logical_or(
                jnp.logical_and(d > 0, d <= z), jnp.logical_and(d == 0, xq > x)
            )

            @pl.when(run)
            def _():
                pair(d, xq, False)

            @pl.when(jnp.logical_not(jnp.logical_or(run, jnp.logical_and(d == 0, xq == x))))
            def _():
                part[d, xq] = jnp.zeros((ROWS, HEAD_DIM), F32)

    pair(0, x, True)

    def local_part():
        cum = cums[...]
        row = cum.T[0:1, :]
        r0 = lax.broadcasted_iota(jnp.int32, (ROWS, ROWS), 0)
        r1 = lax.broadcasted_iota(jnp.int32, (ROWS, ROWS), 1)
        keep = r0 >= r1
        gap = jnp.concatenate([cum, cum, cum], axis=1) - row
        fade = jnp.exp(jnp.where(keep, gap, 0.0))
        inner = jnp.where(keep, dot_t(rq[...], rk[...]) * fade, 0.0).astype(BF16)
        local[...] = dot(inner, rv[...])

    local_part()
    for i in (0, 3, 1, 2):
        qring.wait(i)
        if i in (0, 3):
            qring.onward(i).start()

    quarter = pl.ds(pl.multiple_of(x * 32, 32), 32)

    def plane_sum():
        for copy in dec_out + fresh_out:
            copy.wait_recv()
        state = jnp.zeros((32, HEAD_DIM), F32)
        whole = jnp.zeros((1, HEAD_DIM), F32)
        for k in range(NX):
            own = dec[k][0:1, :]
            state = state * jnp.exp(own) + fresh[k, quarter, :].astype(F32)
            whole = whole + own
        smsg[0, 0:32, :] = state
        smsg[0, 32:40, :] = jnp.broadcast_to(whole, (8, HEAD_DIM))

    s_out = exchange("z", z, NZ, smsg.at[0], lambda me, i: smsg.at[i], s_s, s_r)

    def plane_prefix():
        for copy in s_out:
            copy.wait_recv()
        state = jnp.zeros((32, HEAD_DIM), F32)
        for d in range(NZ - 1, 0, -1):
            state = jnp.where(d <= z, state * jnp.exp(smsg[d, 32:33, :]) + smsg[d, 0:32, :], state)
        stq[x] = state

    q_out = exchange("x", x, NX, stq.at[x], lambda me, i: stq.at[me], x_s.at[2], x_r.at[2])

    def head_view(buf):
        def view(slot, half, core):
            lanes = pl.ds(pl.multiple_of(core * 128, 128), 128)
            return buf.at[slot, pl.ds(HALF * half, HALF), lanes]

        return view

    rring = PairRing(y, c, head_view(rbuf), ret_s.at[0], ret_r.at[0], ret_s.at[1], ret_r.at[1])
    sring = PairRing(y, c, head_view(sbuf), stk_s.at[0], stk_r.at[0], stk_s.at[1], stk_r.at[1])
    own_lanes = pl.ds(pl.multiple_of(c * 128, 128), 128)

    def retention_out():
        for copy in q_out:
            copy.wait_recv()
        state = jnp.concatenate([stq[k] for k in range(NX)], axis=0)
        for k in range(NX - 1):
            nxt = state * jnp.exp(dec[k][0:1, :]) + fresh[k].astype(F32)
            state = jnp.where(k < x, nxt, state)
        hi = state.astype(BF16)
        low = (state - hi.astype(F32)).astype(BF16)
        carried = (dot(rq[...], hi) + dot(rq[...], low)) * jnp.exp(cums[...])
        rbuf[y, :, own_lanes] = head_norm(local[...] + carried).astype(BF16)

    @pl.loop(1, 4)
    def _(k):
        here(kbuf, 0, k)
        up(kbuf, 0, k).start()
        here(kbuf, 0, 8 - k)

        @pl.when(k < 3)
        def _():
            down(kbuf, 0, 8 - k).start()

        @pl.when(k == 1)
        def _():
            qring.wait(4)
            qring.wait(5)

        pairs((9 - k) % 8)
        here(vbuf, 1, k)

        @pl.when(k < 3)
        def _():
            up(vbuf, 1, k).start()

        here(vbuf, 1, 8 - k)
        down(vbuf, 1, 8 - k).start()

        @pl.when(k == 1)
        def _():
            plane_sum()
            for copy in s_out:
                copy.start()

        @pl.when(k == 2)
        def _():
            plane_prefix()
            for copy in q_out:
                copy.start()

        @pl.when(k == 3)
        def _():
            retention_out()
            rring.begin()

        pairs(k)

    here(kbuf, 0, 4)
    here(vbuf, 1, 4)
    rring.pump(0)
    rring.pump(3)

    @pl.loop(0, 2)
    def _(k):
        pairs(5 - k)

    for k in range(NX):
        ttx[x, pl.ds(8 * k, 8), :] = tots[k].T[0:8, :]
    t_out = exchange("x", x, NX, ttx.at[x], lambda me, i: ttx.at[me], x_s.at[3], x_r.at[3])
    for copy in t_out:
        copy.start()
    for i in (1, 2, 4, 5):
        rring.pump(i)
    for copy in weight_copies():
        copy.wait_recv()
    for copy in keep:
        copy.wait()
    for i in (6, 7, 0, 1, 2, 3, 4, 5):
        rring.other(i)
    for copy in t_out:
        copy.wait_recv()

    c_out = []
    for i in range(1, NX):
        to = (x + i) % NX
        c_out.append(
            remote(csend.at[to], crecv.at[x], x_s.at[4, i - 1], x_r.at[4, i - 1], {"x": to})
        )

    def combine(xq):
        rows = pl.ds(pl.multiple_of(8 * xq, 8), 8)
        behind = jnp.zeros((1, ROWS), F32)
        plane = jnp.zeros((8, ROWS), F32)
        after = jnp.zeros((8, ROWS), F32)
        for k in range(NX):
            mine = ttx[k, rows, :]
            plane = plane + mine
            after = jnp.where(k > x, after + mine, after)
        lines = []
        for d in range(NZ):
            lines.append(behind + after[d : d + 1, :])
            behind = behind + plane[d : d + 1, :]
        w = jnp.exp2(-jnp.concatenate(lines, axis=0))
        w = jnp.concatenate([w, jnp.zeros((120, ROWS), F32)], axis=0).T
        value = w[:, 0:1] * part[0, xq]
        for d in range(1, NZ):
            value = value + w[:, d : d + 1] * part[d, xq]
        csend[xq] = value.astype(BF16)

    for i in range(1, NX):
        combine((x + (2, 1, 3)[i - 1]) % NX)
        c_out[(2, 1, 3)[i - 1] - 1].start()
    combine(x)
    acc[:, 0:256] = dot(rbuf[0], owr[0])
    for k in range(1, NY):
        acc[:, 0:256] += dot(rbuf[k], owr[k])
    for copy in c_out:
        copy.wait_recv()
    value = csend[x].astype(F32)
    for i in range(1, NX):
        value = value + crecv[(x + i) % NX].astype(F32)
    sbuf[y, :, own_lanes] = head_norm(value).astype(BF16)
    sring.begin()
    for i in (0, 3, 1, 2):
        sring.pump(i)
    sring.other(6)
    sring.other(7)
    acc[:, 0:256] += dot(sbuf[y], ows[y])
    sring.pump(4)
    sring.pump(5)
    sring.other(0)
    sring.other(1)
    acc[:, 0:256] += dot(sbuf[sring.prv], ows[sring.prv])
    sring.other(2)
    sring.other(3)
    acc[:, 0:256] += dot(sbuf[sring.nxt], ows[sring.nxt])
    sring.other(4)
    sring.other(5)
    out[...] = (acc[:, 0:256] + dot(sbuf[sring.far], ows[sring.far])).astype(BF16)

    qring.drain()
    rring.finish()
    sring.finish()
    for copy in dec_out + fresh_out + s_out + q_out + t_out + c_out + weight_copies():
        copy.wait_send()
    hop(kbuf, 0, 0, 7, zd).wait_send()
    hop(vbuf, 1, 0, 7, zd).wait_send()
    for d in range(0, 4):
        up(kbuf, 0, d).wait_send()
    for d in range(0, 3):
        up(vbuf, 1, d).wait_send()
    for d in (7, 6):
        down(kbuf, 0, d).wait_send()
    for d in (7, 6, 5):
        down(vbuf, 1, d).wait_send()


def body(tokens, rq, rk, rv, sq, sk, sv, log_decay, stick_bias, out_ret, out_stick):
    ct, st, cb, sb = (jnp.asarray(t) for t in angle_tables())
    vmem = pl.BlockSpec(memory_space=pltpu.VMEM)
    anym = pl.BlockSpec(memory_space=pl.ANY)
    smem = pl.BlockSpec(memory_space=pltpu.SMEM)
    v, dma = pltpu.VMEM, pltpu.SemaphoreType.DMA
    return pl.pallas_call(
        kernel,
        out_shape=jax.ShapeDtypeStruct((ROWS, 256), BF16),
        in_specs=[anym, vmem, smem, vmem, vmem] + [anym] * 10,
        out_specs=vmem,
        scratch_shapes=[
            v((NY, ROWS, 512), BF16),
            v((D, 768), BF16),
            v((256, D), BF16),
            v((NY, 256, 256), BF16),
            v((NY, 256, 256), BF16),
            v((2, ROWS, HEAD_DIM), F32),
            v((ROWS, 768), F32),
            v((NX, ROWS, HEAD_DIM), BF16),
            v((NZ, ROWS, HEAD_DIM), BF16),
            v((NZ, ROWS, HEAD_DIM), BF16),
            v((NZ, NX, ROWS, HEAD_DIM), F32),
            v((NX, ROWS, HEAD_DIM), F32),
            v((NX, 32, ROWS), F32),
            v((NX, ROWS, HEAD_DIM), BF16),
            v((NX, ROWS, HEAD_DIM), BF16),
            v((NX, HEAD_DIM, HEAD_DIM), BF16),
            v((NX, 8, HEAD_DIM), F32),
            v((NZ, 40, HEAD_DIM), F32),
            v((NX, 32, HEAD_DIM), F32),
            v((NY, ROWS, 256), BF16),
            v((NY, ROWS, 256), BF16),
            v((ROWS, HEAD_DIM), BF16),
            v((ROWS, HEAD_DIM), BF16),
            v((ROWS, HEAD_DIM), BF16),
            v((ROWS, HEAD_DIM), F32),
            v((ROWS, HEAD_DIM), F32),
            v((256, 384), BF16),
            v((128, 256), BF16),
            dma((13,)),
            dma((2, 8)),
            dma((2, 8)),
            dma((2, 8)),
            dma((2, 8)),
            dma((2, 8)),
            dma((2, 8)),
            dma((6,)),
            dma((6,)),
            dma((2, 8)),
            dma((2, 8)),
            dma((5, 3)),
            dma((5, 3)),
            dma((7,)),
            dma((7,)),
            dma((2, NY, 2)),
            dma((2, NY, 2)),
        ],
        compiler_params=pltpu.CompilerParams(
            collective_id=0, has_side_effects=True, vmem_limit_bytes=48 * 1024 * 1024
        ),
    )(
        tokens,
        log_decay,
        stick_bias,
        cb,
        sb,
        rq,
        rk,
        rv,
        sq,
        sk,
        sv,
        out_ret,
        out_stick,
        ct,
        st,
    )


def solution(mesh):
    grid = Mesh(mesh.devices.reshape(NZ, NX, NY, NC), ("z", "x", "y", "c"))
    return jax.shard_map(
        body,
        mesh=grid,
        in_specs=(
            P(SP, TP),
            P(None, TP),
            P(None, TP),
            P(None, TP),
            P(None, TP),
            P(None, TP),
            P(None, TP),
            P(SP, TP),
            P(TP),
            P(TP, None),
            P(TP, None),
        ),
        out_specs=P(SP, TP),
        check_vma=False,
    )
```

time: 290 us -> 86.3 us (0.30)
  the two profiles are of different devices: /device:TPU:224 before, /device:TPU:193 now
where the time goes in v1:
time: 86.3 us; the launch traced here: 85.6 us
  Pallas kernels  72.3 us (84%)
  local copies, waits for them, and re-layouts  12.5 us (14%)
    pallas_call x1, Pallas kernels, body(): pl.pallas_call(kernel, out_shape=jax.ShapeDtypeStruct((ROWS, 256), BF16),...  72.3 us
    unnamed x30, local copies, waits for them, and re-layouts  12.5 us

profile of v1, /device:TPU:193, one launch (start us, length us, event | category | flops | bytes accessed | tf_op | source)
XLA Modules:
  0.0 85.6 jit_solution(11053451129352100140)
XLA Ops:
  0.0 0.0 copy-start.13
  0.0 0.0 copy-start.8
  0.7 0.0 copy-done.13
  0.7 0.1 copy.16.decays
  0.9 0.1 copy-done.8
  1.0 0.0 copy-start
  1.0 1.0 %copy-done = bf16[2048,128]{1,0:T(8,128)(2,1)S(1)} copy-done((bf16[2048,128]{1,0:T(8,128)(2,1)S(1)}, bf16[2048,128]{1,0:T(8,128)(2,1)}, u32[]{:S(2)}) %copy-start) | copy-done | bytes 524312
  2.0 0.0 copy-start.1
  2.0 1.0 %copy-done.1 = bf16[2048,128]{1,0:T(8,128)(2,1)S(1)} copy-done((bf16[2048,128]{1,0:T(8,128)(2,1)S(1)}, bf16[2048,128]{1,0:T(8,128)(2,1)}, u32[]{:S(2)}) %copy-start.1) | copy-done | bytes 524312
  3.0 0.0 copy-start.2
  3.0 1.0 %copy-done.2 = bf16[2048,128]{1,0:T(8,128)(2,1)S(1)} copy-done((bf16[2048,128]{1,0:T(8,128)(2,1)S(1)}, bf16[2048,128]{1,0:T(8,128)(2,1)}, u32[]{:S(2)}) %copy-start.2) | copy-done | bytes 524312
  4.1 0.0 copy-start.3
  4.1 1.0 %copy-done.3 = bf16[2048,128]{1,0:T(8,128)(2,1)S(1)} copy-done((bf16[2048,128]{1,0:T(8,128)(2,1)S(1)}, bf16[2048,128]{1,0:T(8,128)(2,1)}, u32[]{:S(2)}) %copy-start.3) | copy-done | bytes 524312
  5.1 0.0 copy-start.4
  5.1 1.0 %copy-done.4 = bf16[2048,128]{1,0:T(8,128)(2,1)S(1)} copy-done((bf16[2048,128]{1,0:T(8,128)(2,1)S(1)}, bf16[2048,128]{1,0:T(8,128)(2,1)}, u32[]{:S(2)}) %copy-start.4) | copy-done | bytes 524312
  6.2 0.0 copy-start.5
  6.2 1.0 %copy-done.5 = bf16[2048,128]{1,0:T(8,128)(2,1)S(1)} copy-done((bf16[2048,128]{1,0:T(8,128)(2,1)S(1)}, bf16[2048,128]{1,0:T(8,128)(2,1)}, u32[]{:S(2)}) %copy-start.5) | copy-done | bytes 524312
  7.2 0.0 copy-start.6
  7.2 1.0 %copy-done.6 = bf16[128,2048]{1,0:T(8,128)(2,1)S(1)} copy-done((bf16[128,2048]{1,0:T(8,128)(2,1)S(1)}, bf16[128,2048]{1,0:T(8,128)(2,1)}, u32[]{:S(2)}) %copy-start.6) | copy-done | bytes 524312
  8.3 0.0 copy-start.7
  8.3 1.0 %copy-done.7 = bf16[128,2048]{1,0:T(8,128)(2,1)S(1)} copy-done((bf16[128,2048]{1,0:T(8,128)(2,1)S(1)}, bf16[128,2048]{1,0:T(8,128)(2,1)}, u32[]{:S(2)}) %copy-start.7) | copy-done | bytes 524312
  9.3 0.0 copy-start.9
  9.3 0.9 %copy-done.9 = f32[384,128]{1,0:T(8,128)S(1)} copy-done((f32[384,128]{1,0:T(8,128)S(1)}, f32[384,128]{1,0:T(8,128)}, u32[]{:S(2)}) %copy-start.9) | copy-done | bytes 196632
  10.2 0.0 copy-start.10
  10.2 0.9 %copy-done.10 = f32[384,128]{1,0:T(8,128)S(1)} copy-done((f32[384,128]{1,0:T(8,128)S(1)}, f32[384,128]{1,0:T(8,128)}, u32[]{:S(2)}) %copy-start.10) | copy-done | bytes 196632
  11.2 0.0 copy-start.11
  11.2 0.7 copy-done.11
  11.9 0.0 copy-start.12
  11.9 0.7 copy-done.12
  12.6 72.3 %shard_map.145 = bf16[384,256]{1,0:T(8,128)(2,1)S(1)} custom-call(bf16[384,256]{1,0:T(8,128)(2,1)S(1)} %copy-done.8, f32[384,1]{1,0:T(8,128)S(1)} %copy.16.decays, f32[1]{0:T(128)S(6)} %copy.18.bias, f32[32,128]{1,0:T(8,128)S(1)} %copy-done.12, f32[32,128]{1,0:T(8,128)S(1)} %copy-done.11, bf16[2048,128]{1,0:T(8,128)(2,1)S(1)} %copy-done, ...), custom_call_target="tpu_custom_call" | custom-call | tf_op jit(solution)/shard_map/pallas_call | solution.py:636
  84.9 0.7 copy.19
Async XLA Ops:
  0.0 0.7 copy-start.13
  0.0 1.0 %copy-start.8 = (bf16[384,256]{1,0:T(8,128)(2,1)S(1)}, bf16[384,256]{1,0:T(8,128)(2,1)}, u32[]{:S(2)}) copy-start(bf16[384,256]{1,0:T(8,128)(2,1)} %tokens.1) | copy-start | bytes 589828
  1.0 1.0 %copy-start = (bf16[2048,128]{1,0:T(8,128)(2,1)S(1)}, bf16[2048,128]{1,0:T(8,128)(2,1)}, u32[]{:S(2)}) copy-start(bf16[2048,128]{1,0:T(8,128)(2,1)} %w0.1) | copy-start | bytes 1572868
  2.0 1.0 %copy-start.1 = (bf16[2048,128]{1,0:T(8,128)(2,1)S(1)}, bf16[2048,128]{1,0:T(8,128)(2,1)}, u32[]{:S(2)}) copy-start(bf16[2048,128]{1,0:T(8,128)(2,1)} %w1.1) | copy-start | bytes 1572868
  3.0 1.0 %copy-start.2 = (bf16[2048,128]{1,0:T(8,128)(2,1)S(1)}, bf16[2048,128]{1,0:T(8,128)(2,1)}, u32[]{:S(2)}) copy-start(bf16[2048,128]{1,0:T(8,128)(2,1)} %w2.1) | copy-start | bytes 1572868
  4.1 1.0 %copy-start.3 = (bf16[2048,128]{1,0:T(8,128)(2,1)S(1)}, bf16[2048,128]{1,0:T(8,128)(2,1)}, u32[]{:S(2)}) copy-start(bf16[2048,128]{1,0:T(8,128)(2,1)} %w3.1) | copy-start | bytes 1572868
  5.1 1.0 %copy-start.4 = (bf16[2048,128]{1,0:T(8,128)(2,1)S(1)}, bf16[2048,128]{1,0:T(8,128)(2,1)}, u32[]{:S(2)}) copy-start(bf16[2048,128]{1,0:T(8,128)(2,1)} %w4.1) | copy-start | bytes 1572868
  6.2 1.0 %copy-start.5 = (bf16[2048,128]{1,0:T(8,128)(2,1)S(1)}, bf16[2048,128]{1,0:T(8,128)(2,1)}, u32[]{:S(2)}) copy-start(bf16[2048,128]{1,0:T(8,128)(2,1)} %w5.1) | copy-start | bytes 1572868
  7.2 1.0 %copy-start.6 = (bf16[128,2048]{1,0:T(8,128)(2,1)S(1)}, bf16[128,2048]{1,0:T(8,128)(2,1)}, u32[]{:S(2)}) copy-start(bf16[128,2048]{1,0:T(8,128)(2,1)} %o0.1) | copy-start | bytes 1572868
  8.3 1.0 %copy-start.7 = (bf16[128,2048]{1,0:T(8,128)(2,1)S(1)}, bf16[128,2048]{1,0:T(8,128)(2,1)}, u32[]{:S(2)}) copy-start(bf16[128,2048]{1,0:T(8,128)(2,1)} %o1.1) | copy-start | bytes 1572868
  9.3 0.9 %copy-start.9 = (f32[384,128]{1,0:T(8,128)S(1)}, f32[384,128]{1,0:T(8,128)}, u32[]{:S(2)}) copy-start(f32[384,128]{1,0:T(8,128)} %constant.9.clone.tab_sin) | copy-start | bytes 589828
  10.2 0.9 %copy-start.10 = (f32[384,128]{1,0:T(8,128)S(1)}, f32[384,128]{1,0:T(8,128)}, u32[]{:S(2)}) copy-start(f32[384,128]{1,0:T(8,128)} %constant.8.clone.tab_cos) | copy-start | bytes 589828
  11.2 0.7 copy-start.11
  11.9 0.7 copy-start.12
